TPU v7x, 32 devices: a whole 2x2x4 slice. The times are simulated.
32 devices in a mesh: grp: 2 (over y), sp: 4 (over z), tp: 4 (over x, core).
Axes of the slice: x: 2, y: 2, z: 4, core: 2. Of those that a mesh axis runs over, the one named last changes fastest.
Arguments:
- queries: bfloat16 [2048, 2048], P(('grp', 'sp'), 'tp'), parts along dimension 0, may hold values from -6 to 6
- keys: bfloat16 [2048, 512], P(('grp', 'sp'), 'tp'), parts along dimension 0, may hold values from -6 to 6
- values: bfloat16 [2048, 512], P(('grp', 'sp'), 'tp'), parts along dimension 0, may hold values from -6 to 6
- query_gain: float32 [128], replicated, may hold values from 1 to 5, as said below
- key_norm_gain: float32 [128], replicated, may hold values from 1 to 5, as said below
- out_weight: bfloat16 [2048, 2048], P('tp'), may hold values from -0.125 to 0.125
- residual: bfloat16 [2048, 2048], P(('grp', 'sp')), parts along dimension 0, may hold values from -0.59765625 to 0.59765625
- mixer_gain: float32 [2048], replicated, may hold values from 0.1 to 1.9
- gate_weight: bfloat16 [2048, 5632], P('sp', 'tp'), may hold values from -0.125 to 0.125
- up_weight: bfloat16 [2048, 5632], P('sp', 'tp'), may hold values from -0.125 to 0.125
- conv_taps: float32 [3, 5632], P(None, 'tp'), may hold values from -3.5 to 3.5
- down_weight: bfloat16 [5632, 2048], P('tp', 'sp'), may hold values from -0.078125 to 0.078125
Outputs:
- layer_out: bfloat16 [2048, 2048], P(('grp', 'sp', 'tp')), parts along dimension 0
There are 2 independent parts, one for each index of `grp`. A program takes and returns all parts, laid end to end along the dimension named above; an argument that names none is the same for every part. Nothing has to cross between parts.
Inputs may be any that keep to these rules, and one draw needn't show every extreme that they name: `query_gain`: positive. `key_norm_gain`: positive.
All inputs are finite; a program needn't handle non-finite values.
Results may differ from a plain program's by a relative error of at most 0.024.
Values may be sent and summed in bfloat16 or wider, within the bound.
A program may use at most 128 MiB of HBM per device.

v0:
```python
import math
import jax
import jax.numpy as jnp
from jax import lax
from jax.sharding import PartitionSpec as P

GRID = 64
norm_eps = 1e-06
rope_base = 10000.0


def padded_2(block, sides, width):
    for axis, dim in sides:
        count = lax.axis_size(axis)
        forward = [(i, i + 1) for i in range(count - 1)]
        backward = [(target, source) for source, target in forward]
        low = lax.ppermute(
            lax.slice_in_dim(block, block.shape[dim] - width, None, axis=dim), axis, forward
        )
        high = lax.ppermute(lax.slice_in_dim(block, 0, width, axis=dim), axis, backward)
        block = jnp.concatenate([low, block, high], axis=dim)
    return block


def angle_tables(positions, head_dim):
    quarter = head_dim // 4
    freqs = 1.0 / rope_base ** (jnp.arange(quarter, dtype=jnp.float32) * 4.0 / head_dim)
    grid_row = (positions // GRID).astype(jnp.float32)
    grid_col = (positions % GRID).astype(jnp.float32)
    by_row = grid_row[:, None] * freqs[None, :]
    by_col = grid_col[:, None] * freqs[None, :]
    angles = jnp.concatenate([by_row, by_row, by_col, by_col], axis=-1)
    return (jnp.cos(angles), jnp.sin(angles))


def apply_rotary(field, cosine_table, sine_table):
    half = field.shape[-1] // 2
    quarter = half // 2
    first = field[..., :half]
    second = field[..., half:]
    turned = jnp.concatenate(
        [
            -first[..., quarter:],
            first[..., :quarter],
            -second[..., quarter:],
            second[..., :quarter],
        ],
        axis=-1,
    )
    return field * cosine_table[:, None, :] + turned * sine_table[:, None, :]


def per_head_norm(field, gain):
    floats = field.astype(jnp.float32)
    return floats * lax.rsqrt(jnp.mean(floats * floats, axis=-1, keepdims=True) + norm_eps) * gain


def local(
    queries,
    keys,
    values,
    query_gain,
    key_norm_gain,
    out_weight,
    residual,
    mixer_gain,
    gate_weight,
    up_weight,
    conv_taps,
    down_weight,
):
    tok_rows = queries.shape[0]
    head_dim = query_gain.shape[0]
    heads_here = queries.shape[1] // head_dim
    kv_here = keys.shape[1] // head_dim
    query_group = heads_here // kv_here
    part_rows = tok_rows // lax.axis_size("tp")
    positions = lax.axis_index("sp") * tok_rows + jnp.arange(tok_rows, dtype=jnp.int32)
    cosine_table, sine_table = angle_tables(positions, head_dim)
    rotated_queries = apply_rotary(
        per_head_norm(queries.reshape(tok_rows, heads_here, head_dim), query_gain),
        cosine_table,
        sine_table,
    ).astype(jnp.bfloat16)
    rotated_keys = apply_rotary(
        per_head_norm(keys.reshape(tok_rows, kv_here, head_dim), key_norm_gain),
        cosine_table,
        sine_table,
    ).astype(jnp.bfloat16)
    key_flat = rotated_keys.reshape(tok_rows, kv_here * head_dim)
    query_mat = jnp.transpose(
        rotated_queries.reshape(tok_rows, kv_here, query_group, head_dim), (1, 2, 0, 3)
    )
    query_mat = query_mat.reshape(kv_here, query_group * tok_rows, head_dim)
    scale = head_dim ** (-0.5)
    start_state = (
        jnp.full((kv_here, query_group * tok_rows), -jnp.inf, jnp.float32),
        jnp.zeros((kv_here, query_group * tok_rows), jnp.float32),
        jnp.zeros((kv_here, query_group * tok_rows, head_dim), jnp.float32),
    )
    key_piece = lax.all_gather(key_flat, "sp", axis=0, tiled=True)
    value_piece = lax.all_gather(values, "sp", axis=0, tiled=True)
    piece_rows = key_piece.shape[0]
    block_slice = math.gcd(piece_rows, 512)
    key_blocks = key_piece.reshape(piece_rows // block_slice, block_slice, kv_here, head_dim)
    value_blocks = value_piece.reshape(piece_rows // block_slice, block_slice, kv_here, head_dim)

    def one_block(state, block_pair):
        running, totals, accum = state
        key_block, value_block = block_pair
        scores = (
            jnp.einsum("hqd,khd->hqk", query_mat, key_block, preferred_element_type=jnp.float32)
            * scale
        )
        new_max = jnp.maximum(running, jnp.max(scores, axis=-1))
        factor = jnp.exp(running - new_max)
        expo = jnp.exp(scores - new_max[..., None])
        totals = totals * factor + jnp.sum(expo, axis=-1)
        accum = accum * factor[..., None] + jnp.einsum(
            "hqk,khd->hqd",
            expo.astype(jnp.bfloat16),
            value_block,
            preferred_element_type=jnp.float32,
        )
        return ((new_max, totals, accum), None)

    result, unused = lax.scan(one_block, start_state, (key_blocks, value_blocks))
    running, totals, accum = result
    heads = (accum / totals[..., None]).astype(jnp.bfloat16)
    heads = jnp.transpose(heads.reshape(kv_here, query_group, tok_rows, head_dim), (2, 0, 1, 3))
    heads = heads.reshape(tok_rows, heads_here * head_dim)
    own_start = lax.axis_index("tp") * part_rows
    full_proj = lax.psum(
        jnp.dot(heads, out_weight, preferred_element_type=jnp.float32).astype(jnp.bfloat16), "tp"
    ).astype(jnp.float32)
    mixed = residual.astype(jnp.float32) + full_proj
    normed = per_head_norm(mixed, mixer_gain).astype(jnp.bfloat16)
    mixed_keep = lax.dynamic_slice_in_dim(mixed, own_start, part_rows, 0)
    gate_acc = jnp.dot(
        normed,
        lax.all_gather(gate_weight, "sp", axis=0, tiled=True),
        preferred_element_type=jnp.float32,
    )
    up_acc = jnp.dot(
        normed,
        lax.all_gather(up_weight, "sp", axis=0, tiled=True),
        preferred_element_type=jnp.float32,
    )
    gate = gate_acc.astype(jnp.bfloat16)
    up_val = up_acc.astype(jnp.bfloat16)
    padded = padded_2(gate, (("sp", 0),), 1).astype(jnp.float32)
    conv = conv_taps[0] * padded[:-2] + conv_taps[1] * padded[1:-1] + conv_taps[2] * padded[2:]
    hidden = (jax.nn.silu(conv) * up_val.astype(jnp.float32)).astype(jnp.bfloat16)
    down_full = lax.all_gather(down_weight, "sp", axis=1, tiled=True)
    mixer_out = lax.psum_scatter(
        jnp.dot(hidden, down_full, preferred_element_type=jnp.float32).astype(jnp.bfloat16),
        "tp",
        scatter_dimension=0,
        tiled=True,
    ).astype(jnp.float32)
    return (mixed_keep + mixer_out).astype(jnp.bfloat16)


def solution(mesh):
    in_specs = (
        P(("grp", "sp"), "tp"),
        P(("grp", "sp"), "tp"),
        P(("grp", "sp"), "tp"),
        P(),
        P(),
        P("tp", None),
        P(("grp", "sp"), None),
        P(),
        P("sp", "tp"),
        P("sp", "tp"),
        P(None, "tp"),
        P("tp", "sp"),
    )
    out_specs = P(("grp", "sp", "tp"), None)
    return jax.shard_map(local, mesh=mesh, in_specs=in_specs, out_specs=out_specs, check_vma=False)
```

profile of v0, /device:TPU:0, one launch (start us, length us, event | category | flops | bytes accessed | tf_op | source)
XLA Modules:
  0.0 424.0 jit_solution(16997622798966750573)
XLA Ops:
  7.4 0.0 copy-start
  7.4 0.0 all-reduce.2.cloned.1.call-start
  7.4 1.3 reshape.324
  8.7 1.9 reshape.323
  10.6 1.0 fusion.32
  11.5 0.9 fusion.34
  12.5 0.2 fusion.39
  12.7 0.3 multiply_reduce_fusion.2
  13.0 0.0 copy-done.7
  13.1 0.3 multiply_multiply_fusion
  13.4 0.0 copy-start.3
  13.4 0.0 copy-start.6
  13.4 0.0 copy-start.2
  13.4 0.9 fusion.28
  14.3 0.1 broadcast_multiply_fusion.1
  14.5 0.0 copy-done.3
  14.5 0.0 copy-done.6
  14.5 0.6 fusion.37
  15.1 0.0 copy-start.4
  15.1 0.0 copy-done.2
  15.2 1.2 fusion.31
  16.4 15.7 %all_gather.15 = bf16[1024,128]{1,0:T(8,128)(2,1)S(1)} all-gather(bf16[256,128]{1,0:T(8,128)(2,1)S(1)} %get-tuple-element.109), channel_id=1, replica_groups=mesh['grp'=2,'sp'=4,'tp'=4] {'sp'}, dimensions={0}, use_global_device_ids=true | all-gather | bytes 327680 | tf_op jit(solution)/shard_map/all_gather | solution.py:101
  32.0 0.0 copy-done.4
  32.0 14.6 %all_gather.16 = bf16[1024,128]{1,0:T(8,128)(2,1)S(1)} all-gather(bf16[256,128]{1,0:T(8,128)(2,1)S(1)} %copy-done.4), channel_id=1, replica_groups=mesh['grp'=2,'sp'=4,'tp'=4] {'sp'}, dimensions={0}, use_global_device_ids=true | all-gather | bytes 327680 | tf_op jit(solution)/shard_map/all_gather | solution.py:102
  46.6 9.3 %while.15 = (s32[]{:T(128)}, f32[1,1024]{1,0:T(1,128)S(1)}, f32[1,1024]{1,0:T(1,128)S(1)}, f32[1,1024,128]{2,1,0:T(8,128)S(1)}, bf16[2,512,1,128]{3,1,2,0:T(8,12...) while((s32[]{:T(128)}, f32[1,1024]{1,0:T(1,128)S(1)}, ...), condition=%wide.region_5.6_spmd.clone, body=%wide.region_2.5_spmd.clone.sunk | while | flops 273028096 | bytes 16318605 | solution.py:127
  46.6 1.8 multiply_reduce_fusion.4
  48.4 2.1 fusion.63
  50.5 0.1 copy-done.1
  50.6 0.6 fusion.65
  51.3 1.8 multiply_reduce_fusion.4
  53.1 2.1 fusion.63
  55.2 0.1 copy-done.1
  55.3 0.6 fusion.65
  55.9 0.2 divide_convert_fusion
  56.1 0.1 copy.27
  56.3 0.0 copy-done
  56.3 1.7 convolution_convert_fusion
  58.0 0.0 all-reduce.2.cloned.1.call-update
  58.0 0.0 all-gather.4.cloned.1.call-start
  58.1 0.5 all-gather.4.cloned.1.call-update
  58.6 0.0 all-gather.6.cloned.1.call-start
  58.7 0.5 all-gather.6.cloned.1.call-update
  59.2 0.0 all-gather.8.cloned.1.call-start
  59.2 0.5 all-gather.8.cloned.1.call-update
  59.8 0.0 copy-start.8
  59.8 0.0 reduce-scatter.2.cloned.1.call-start
  59.8 35.8 %all-reduce.2.cloned.1.call-done = bf16[256,2048]{1,0:T(8,128)(2,1)} async-done(((bf16[256,2048]{1,0:T(8,128)(2,1)}), bf16[256,2048]{1,0:T(8,128)(2,1)}) %all-reduce.2.cloned.1.call-update) | async-done | bytes 1048592 | tf_op jit(solution)/shard_map/psum | solution.py:133
  95.7 3.2 convert_add_fusion
  98.9 68.7 %all-gather.4.cloned.1.call-done = bf16[2048,1408]{1,0:T(8,128)(2,1)} async-done(((bf16[512,1408]{1,0:T(8,128)(2,1)}), bf16[2048,1408]{1,0:T(8,128)(2,1)}) %all-gather.4.cloned.1.call-update) | async-done | bytes 5767184 | tf_op jit(solution)/shard_map/all_gather | solution.py:141
  167.6 0.0 copy-done.8
  167.6 5.1 %convolution_convert_fusion.2 = bf16[256,1408]{1,0:T(8,128)(2,1)S(1)} fusion(bf16[2048,1408]{1,0:T(8,128)(2,1)} %all-gather.4.cloned.1.call-done, f32[2048]{0:T(1024)S(1)} %copy-done.8, f32[256]{0:T(256)S(1)} %add_rsqrt_fusion.1, bf16[256,2048]{1,0:T(8,128)(2,1)} %all-reduce.2.cloned.1.call-done, bf16[256,2048]{1,0:T(8,128)(2,1)} %param.20), kind=kOutput, calls=%fused_computation.29 | convolution fusion | flops 1479901184 | bytes 8594432 | tf_op jit(solution)/shard_map/dot_general | solution.py:139
  172.8 1.3 collective-permute-start
  174.1 1.5 collective-permute-start.1
  175.6 0.0 copy-done.5
  175.6 0.1 slice_reduce_fusion.2
  175.6 0.0 collective-permute-done
  175.6 4.0 collective-permute-done.1
  179.6 1.3 maximum_convert_fusion
  180.9 93.1 %all-gather.6.cloned.1.call-done = bf16[2048,1408]{1,0:T(8,128)(2,1)} async-done(((bf16[512,1408]{1,0:T(8,128)(2,1)}), bf16[2048,1408]{1,0:T(8,128)(2,1)}) %all-gather.6.cloned.1.call-update) | async-done | bytes 5767184 | tf_op jit(solution)/shard_map/all_gather | solution.py:146
  274.0 106.2 %all-gather.8.cloned.1.call-done = bf16[1408,2048]{1,0:T(8,128)(2,1)} async-done(((bf16[1408,512]{1,0:T(8,128)(2,1)}), bf16[1408,2048]{1,0:T(8,128)(2,1)}) %all-gather.8.cloned.1.call-update) | async-done | bytes 5767184 | tf_op jit(solution)/shard_map/all_gather | solution.py:154
  380.2 11.1 %convolution_convert_fusion.3 = bf16[256,2048]{1,0:T(8,128)(2,1)} fusion(bf16[1408,2048]{1,0:T(8,128)(2,1)} %all-gather.8.cloned.1.call-done, bf16[2048,1408]{1,0:T(8,128)(2,1)} %all-gather.6.cloned.1.call-done, f32[258,1408]{1,0:T(8,128)} %maximum_convert_fusion, f32[1408]{0:T(1024)S(1)} %get-tuple-element.91, f32[1408]{0:T(1024)S(1)} %get-tuple-element.92, ...), kind=kOutput, calls=%fused_computation.30 | convolution fusion | flops 2961145856 | bytes 19031552 | tf_op jit(solution)/shard_map/dot_general | solution.py:156
  391.3 0.0 reduce-scatter.2.cloned.1.call-update
  391.3 23.2 %reduce-scatter.2.cloned.1.call-done = bf16[64,2048]{1,0:T(8,128)(2,1)} async-done(((bf16[256,2048]{1,0:T(8,128)(2,1)}), bf16[64,2048]{1,0:T(8,128)(2,1)}) %reduce-scatter.2.cloned.1.call-update) | async-done | bytes 262160 | tf_op jit(solution)/shard_map/reduce_scatter | solution.py:155
  414.5 1.9 add_convert_fusion
  (20 shorter events, 0.2 us)
Async XLA Ops:
  7.4 48.9 %copy-start = (bf16[512,2048]{1,0:T(8,128)(2,1)S(1)}, bf16[512,2048]{1,0:T(8,128)(2,1)}, u32[]{:S(2)}) copy-start(bf16[512,2048]{1,0:T(8,128)(2,1)} %param.19) | copy-start | bytes 6291460
  7.4 5.7 %copy-start.7 = (f32[128]{0:T(128)S(1)}, f32[128]{0:T(128)}, u32[]{:S(2)}) copy-start(f32[128]{0:T(128)} %param.17) | copy-start | bytes 1540
  7.4 88.3 %all-reduce.2.cloned.1.call-start = ((), (), s32[]{:S(2)}) async-start(), calls=%async_computation.1 | async-start | bytes 2097152 | tf_op jit(solution)/shard_map/psum | solution.py:133
  13.4 1.1 copy-start.3
  13.4 1.1 copy-start.6
  13.4 1.7 copy-start.2
  15.1 16.9 %copy-start.4 = (bf16[256,128]{1,0:T(8,128)(2,1)S(1)}, bf16[256,128]{1,0:T(8,128)(2,1)}, u32[]{:S(2)}) copy-start(bf16[256,128]{1,0:T(8,128)(2,1)} %param.16) | copy-start | bytes 196612
  48.4 2.2 copy-start.1
  53.0 2.2 copy-start.1
  58.0 109.6 %all-gather.4.cloned.1.call-start = ((), (), s32[]{:S(2)}) async-start(), calls=%async_computation.2 | async-start | bytes 7208960 | tf_op jit(solution)/shard_map/all_gather | solution.py:141
  58.6 215.4 %all-gather.6.cloned.1.call-start = ((), (), s32[]{:S(2)}) async-start(), calls=%async_computation.3 | async-start | bytes 7208960 | tf_op jit(solution)/shard_map/all_gather | solution.py:146
  59.2 321.0 %all-gather.8.cloned.1.call-start = ((), (), s32[]{:S(2)}) async-start(), calls=%async_computation.4 | async-start | bytes 7208960 | tf_op jit(solution)/shard_map/all_gather | solution.py:154
  59.8 107.8 %copy-start.8 = (f32[2048]{0:T(1024)S(1)}, f32[2048]{0:T(1024)}, u32[]{:S(2)}) copy-start(f32[2048]{0:T(1024)} %param.21) | copy-start | bytes 24580
  59.8 354.7 %reduce-scatter.2.cloned.1.call-start = ((), (), s32[]{:S(2)}) async-start(), calls=%async_computation.5 | async-start | bytes 1310720 | tf_op jit(solution)/shard_map/reduce_scatter | solution.py:155
  98.9 76.6 %copy-start.5 = (f32[3,1408]{1,0:T(4,128)S(1)}, f32[3,1408]{1,0:T(4,128)}, u32[]{:S(2)}) copy-start(f32[3,1408]{1,0:T(4,128)} %param.24) | copy-start | bytes 50692
  172.8 2.8 collective-permute-start
  174.1 5.5 %collective-permute-start.1 = (bf16[1,1408]{1,0:T(2,128)(2,1)S(1)}, bf16[1,1408]{1,0:T(2,128)(2,1)S(1)}, u32[]{:S(2)}, u32[]{:S(2)}) collective-permute-start(bf16[1,1408]{1,0:T(2,128)(2,1)S(1)} %get-tuple-element.117), channel_id=1, source_target_pairs={{4,0},{8,4},{12,8},{5,1},{9,5},{13,9},{6,2},{10,6},{14,10},{7,3},{... | collective-permute-start | bytes 8456 | tf_op jit(solution)/shard_map/ppermute | solution.py:20
Sparse Core Ops, SparseCore 0:
  58.1 37.4 all-reduce.1
  391.4 23.0 reduce-scatter.1
Sparse Core Ops, SparseCore 1:
  60.1 107.5 all-gather.3
  169.0 104.9 all-gather.5
  275.4 104.7 all-gather.7
where the time goes:
time: 424 us
  waiting for transfers between devices  333 us (79%)
  blocking collectives  30.2 us (7%)
  matrix products  22.8 us (5%)
  other arithmetic  16.5 us (4%)
  between operations  15.3 us (4%)
    all_gather x1, waiting for transfers between devices, local(): down_full = lax.all_gather(down_weight, 'sp', axis=1, tiled=True)  106 us
    all_gather x1, waiting for transfers between devices, local(): lax.all_gather(up_weight, 'sp', axis=0, tiled=True)  93.1 us
    all_gather x1, waiting for transfers between devices, local(): lax.all_gather(gate_weight, 'sp', axis=0, tiled=True)  68.7 us
    psum x1, waiting for transfers between devices, local(): lax.psum(jnp.dot(heads, out_weight, preferred_element_type=jnp.float32).a...  35.8 us
    reduce_scatter x1, waiting for transfers between devices, local(): lax.psum_scatter(jnp.dot(hidden, down_full, preferred_element_type=jnp.fl...  23.2 us
    all_gather x1, blocking collectives, local(): key_piece = lax.all_gather(key_flat, 'sp', axis=0, tiled=True)  15.7 us
    all_gather x1, blocking collectives, local(): value_piece = lax.all_gather(values, 'sp', axis=0, tiled=True)  14.6 us
    dot_general x1, matrix products, local(): jnp.dot(hidden, down_full, preferred_element_type=jnp.float32)  11.1 us
  transfers between devices with their start and end apart: 7, of which 6 were waited for; matrix products, arithmetic and copies ran while one was open for 2% of the time, Pallas kernels for 0%

commit v1 on v0

--- a/solution.py
+++ b/solution.py
@@ -7,6 +7,12 @@
 GRID = 64
 norm_eps = 1e-06
 rope_base = 10000.0
+
+
+def gather_and_add(x, axis):
+    parts = lax.all_gather(x, axis, axis=0, tiled=False)
+    result = parts.sum(axis=0)
+    return result
 
 
 def padded_2(block, sides, width):
@@ -130,7 +136,7 @@
     heads = jnp.transpose(heads.reshape(kv_here, query_group, tok_rows, head_dim), (2, 0, 1, 3))
     heads = heads.reshape(tok_rows, heads_here * head_dim)
     own_start = lax.axis_index("tp") * part_rows
-    full_proj = lax.psum(
+    full_proj = gather_and_add(
         jnp.dot(heads, out_weight, preferred_element_type=jnp.float32).astype(jnp.bfloat16), "tp"
     ).astype(jnp.float32)
     mixed = residual.astype(jnp.float32) + full_proj

time: 424 us -> 457 us (1.078)
  waiting for transfers between devices: 333 us -> 363 us
    psum x1 -> x0, waiting for transfers between devices: 35.8 us -> none  [local(): lax.psum(jnp.dot(heads, out_weight, preferred_element_type=jnp.float32).a...]
    all_gather x0 -> x1, waiting for transfers between devices: none -> 33.4 us  [gather_and_add(): parts = lax.all_gather(x, axis, axis=0, tiled=False)]
    all_gather x1, waiting for transfers between devices: 68.7 us -> 101 us  [local(): lax.all_gather(gate_weight, 'sp', axis=0, tiled=True)]
    all_gather x1, waiting for transfers between devices: 93.1 us -> 106 us  [local(): lax.all_gather(up_weight, 'sp', axis=0, tiled=True)]
    all_gather x1, waiting for transfers between devices: 106 us -> 93.3 us  [local(): down_full = lax.all_gather(down_weight, 'sp', axis=1, tiled=True)]
  transfers between devices with their start and end apart: 7 -> 7, of which waited for: 6 -> 6; matrix products, arithmetic and copies ran while one was open for 2% -> 3% of each run, Pallas kernels for 0% -> 0%
where the time goes in v1:
time: 457 us
  waiting for transfers between devices  363 us (79%)
  blocking collectives  30.2 us (7%)
  matrix products  22.8 us (5%)
  other arithmetic  20.8 us (5%)
  between operations  13.4 us (3%)
    all_gather x1, waiting for transfers between devices, local(): lax.all_gather(up_weight, 'sp', axis=0, tiled=True)  106 us
    all_gather x1, waiting for transfers between devices, local(): lax.all_gather(gate_weight, 'sp', axis=0, tiled=True)  101 us
    all_gather x1, waiting for transfers between devices, local(): down_full = lax.all_gather(down_weight, 'sp', axis=1, tiled=True)  93.3 us
    all_gather x1, waiting for transfers between devices, gather_and_add(): parts = lax.all_gather(x, axis, axis=0, tiled=False)  33.4 us
    reduce_scatter x1, waiting for transfers between devices, local(): lax.psum_scatter(jnp.dot(hidden, down_full, preferred_element_type=jnp.fl...  23.2 us
    all_gather x1, blocking collectives, local(): key_piece = lax.all_gather(key_flat, 'sp', axis=0, tiled=True)  15.7 us
    all_gather x1, blocking collectives, local(): value_piece = lax.all_gather(values, 'sp', axis=0, tiled=True)  14.6 us
    dot_general x1, matrix products, local(): jnp.dot(hidden, down_full, preferred_element_type=jnp.float32)  11 us
  transfers between devices with their start and end apart: 7, of which 6 were waited for; matrix products, arithmetic and copies ran while one was open for 3% of the time, Pallas kernels for 0%

profile of v1, /device:TPU:0, one launch (start us, length us, event | category | flops | bytes accessed | tf_op | source)
XLA Modules:
  0.0 456.7 jit_solution(18411397507224111477)
XLA Ops:
  6.5 0.0 copy-start
  6.5 0.0 all-gather.12.cloned.1.call-start
  6.6 1.3 reshape.324
  7.8 1.9 reshape.323
  9.7 1.0 fusion.32
  10.7 0.9 fusion.34
  11.7 0.2 fusion.39
  11.8 0.3 multiply_reduce_fusion.2
  12.2 0.0 copy-done.7
  12.2 0.3 multiply_multiply_fusion
  12.6 0.0 copy-start.3
  12.6 0.0 copy-start.6
  12.6 0.0 copy-start.2
  12.6 0.9 fusion.28
  13.5 0.1 broadcast_multiply_fusion.1
  13.6 0.0 copy-done.3
  13.6 0.0 copy-done.6
  13.6 0.6 fusion.37
  14.3 0.0 copy-start.4
  14.3 0.0 copy-done.2
  14.3 1.2 fusion.31
  15.5 15.7 %all_gather.21 = bf16[1024,128]{1,0:T(8,128)(2,1)S(1)} all-gather(bf16[256,128]{1,0:T(8,128)(2,1)S(1)} %get-tuple-element.109), channel_id=1, replica_groups=mesh['grp'=2,'sp'=4,'tp'=4] {'sp'}, dimensions={0}, use_global_device_ids=true | all-gather | bytes 327680 | tf_op jit(solution)/shard_map/all_gather | solution.py:107
  31.2 0.0 copy-done.4
  31.2 14.6 %all_gather.22 = bf16[1024,128]{1,0:T(8,128)(2,1)S(1)} all-gather(bf16[256,128]{1,0:T(8,128)(2,1)S(1)} %copy-done.4), channel_id=1, replica_groups=mesh['grp'=2,'sp'=4,'tp'=4] {'sp'}, dimensions={0}, use_global_device_ids=true | all-gather | bytes 327680 | tf_op jit(solution)/shard_map/all_gather | solution.py:108
  45.8 9.3 %while.15 = (s32[]{:T(128)}, f32[1,1024]{1,0:T(1,128)S(1)}, f32[1,1024]{1,0:T(1,128)S(1)}, f32[1,1024,128]{2,1,0:T(8,128)S(1)}, bf16[2,512,1,128]{3,1,2,0:T(8,12...) while((s32[]{:T(128)}, f32[1,1024]{1,0:T(1,128)S(1)}, ...), condition=%wide.region_5.6_spmd.clone, body=%wide.region_2.5_spmd.clone.sunk | while | flops 273028096 | bytes 16318605 | solution.py:133
  45.8 1.8 multiply_reduce_fusion.4
  47.6 2.1 fusion.63
  49.7 0.1 copy-done.1
  49.8 0.6 fusion.65
  50.4 1.8 multiply_reduce_fusion.4
  52.2 2.1 fusion.63
  54.4 0.1 copy-done.1
  54.4 0.6 fusion.65
  55.1 0.2 divide_convert_fusion
  55.3 0.1 copy.27
  55.5 0.0 copy-done
  55.5 1.7 convolution_convert_fusion
  57.2 0.0 all-gather.12.cloned.1.call-update
  57.2 0.0 all-gather.6.cloned.1.call-start
  57.3 0.7 all-gather.6.cloned.1.call-update
  58.0 0.0 all-gather.10.cloned.1.call-start
  58.0 0.7 all-gather.10.cloned.1.call-update
  58.7 0.0 all-gather.8.cloned.1.call-start
  58.8 0.5 all-gather.8.cloned.1.call-update
  59.3 0.0 reduce-scatter.2.cloned.1.call-start
  59.3 33.4 %all-gather.12.cloned.1.call-done = bf16[1024,2048]{1,0:T(8,128)(2,1)} async-done(((bf16[256,2048]{1,0:T(8,128)(2,1)}), bf16[1024,2048]{1,0:T(8,128)(2,1)}) %all-gather.12.cloned.1.call-update) | async-done | bytes 4194320 | tf_op jit(solution)/shard_map/all_gather | solution.py:13
  92.8 4.3 reduce_sum.52
  97.1 3.2 convert_add_fusion
  100.3 100.7 %all-gather.6.cloned.1.call-done = bf16[2048,1408]{1,0:T(8,128)(2,1)} async-done(((bf16[512,1408]{1,0:T(8,128)(2,1)}), bf16[2048,1408]{1,0:T(8,128)(2,1)}) %all-gather.6.cloned.1.call-update) | async-done | bytes 5767184 | tf_op jit(solution)/shard_map/all_gather | solution.py:147
  201.1 0.0 copy-done.8
  201.1 5.2 %convolution_convert_fusion.2 = bf16[256,1408]{1,0:T(8,128)(2,1)S(1)} fusion(bf16[2048,1408]{1,0:T(8,128)(2,1)} %all-gather.6.cloned.1.call-done, f32[2048]{0:T(1024)S(1)} %copy-done.8, f32[256]{0:T(256)S(1)} %add_rsqrt_fusion.1, bf16[256,2048]{1,0:T(8,128)(2,1)} %reduce_sum.52, bf16[256,2048]{1,0:T(8,128)(2,1)} %param.20), kind=kOutput, calls=%fused_computation.29 | convolution fusion | flops 1479901184 | bytes 8594432 | tf_op jit(solution)/shard_map/dot_general | solution.py:145
  206.3 1.3 collective-permute-start
  207.6 1.5 collective-permute-start.1
  209.0 0.0 copy-done.5
  209.0 0.1 slice_reduce_fusion.2
  209.1 0.0 collective-permute-done
  209.1 4.0 collective-permute-done.1
  213.1 1.3 maximum_convert_fusion
  214.4 93.3 %all-gather.10.cloned.1.call-done = bf16[1408,2048]{1,0:T(8,128)(2,1)} async-done(((bf16[1408,512]{1,0:T(8,128)(2,1)}), bf16[1408,2048]{1,0:T(8,128)(2,1)}) %all-gather.10.cloned.1.call-update) | async-done | bytes 5767184 | tf_op jit(solution)/shard_map/all_gather | solution.py:160
  307.7 106.4 %all-gather.8.cloned.1.call-done = bf16[2048,1408]{1,0:T(8,128)(2,1)} async-done(((bf16[512,1408]{1,0:T(8,128)(2,1)}), bf16[2048,1408]{1,0:T(8,128)(2,1)}) %all-gather.8.cloned.1.call-update) | async-done | bytes 5767184 | tf_op jit(solution)/shard_map/all_gather | solution.py:152
  414.0 11.0 %convolution_convert_fusion.3 = bf16[256,2048]{1,0:T(8,128)(2,1)} fusion(bf16[1408,2048]{1,0:T(8,128)(2,1)} %all-gather.10.cloned.1.call-done, bf16[2048,1408]{1,0:T(8,128)(2,1)} %all-gather.8.cloned.1.call-done, f32[258,1408]{1,0:T(8,128)} %maximum_convert_fusion, f32[1408]{0:T(1024)S(1)} %get-tuple-element.91, f32[1408]{0:T(1024)S(1)} %get-tuple-element.92, ...), kind=kOutput, calls=%fused_computation.30 | convolution fusion | flops 2961145856 | bytes 19031552 | tf_op jit(solution)/shard_map/dot_general | solution.py:162
  425.1 0.0 reduce-scatter.2.cloned.1.call-update
  425.1 23.2 %reduce-scatter.2.cloned.1.call-done = bf16[64,2048]{1,0:T(8,128)(2,1)} async-done(((bf16[256,2048]{1,0:T(8,128)(2,1)}), bf16[64,2048]{1,0:T(8,128)(2,1)}) %reduce-scatter.2.cloned.1.call-update) | async-done | bytes 262160 | tf_op jit(solution)/shard_map/reduce_scatter | solution.py:161
  448.3 1.9 add_convert_fusion
  (21 shorter events, 0.2 us)
Async XLA Ops:
  6.5 48.9 %copy-start = (bf16[512,2048]{1,0:T(8,128)(2,1)S(1)}, bf16[512,2048]{1,0:T(8,128)(2,1)}, u32[]{:S(2)}) copy-start(bf16[512,2048]{1,0:T(8,128)(2,1)} %param.19) | copy-start | bytes 6291460
  6.5 5.7 %copy-start.7 = (f32[128]{0:T(128)S(1)}, f32[128]{0:T(128)}, u32[]{:S(2)}) copy-start(f32[128]{0:T(128)} %param.17) | copy-start | bytes 1540
  6.5 86.2 %all-gather.12.cloned.1.call-start = ((), (), s32[]{:S(2)}) async-start(), calls=%async_computation.5 | async-start | bytes 5242880 | tf_op jit(solution)/shard_map/all_gather | solution.py:13
  12.6 1.1 copy-start.3
  12.6 1.1 copy-start.6
  12.6 1.7 copy-start.2
  14.3 16.9 %copy-start.4 = (bf16[256,128]{1,0:T(8,128)(2,1)S(1)}, bf16[256,128]{1,0:T(8,128)(2,1)}, u32[]{:S(2)}) copy-start(bf16[256,128]{1,0:T(8,128)(2,1)} %param.16) | copy-start | bytes 196612
  47.5 2.2 copy-start.1
  52.2 2.2 copy-start.1
  57.2 143.8 %all-gather.6.cloned.1.call-start = ((), (), s32[]{:S(2)}) async-start(), calls=%async_computation.1 | async-start | bytes 7208960 | tf_op jit(solution)/shard_map/all_gather | solution.py:147
  58.0 249.7 %all-gather.10.cloned.1.call-start = ((), (), s32[]{:S(2)}) async-start(), calls=%async_computation.3 | async-start | bytes 7208960 | tf_op jit(solution)/shard_map/all_gather | solution.py:160
  58.7 355.3 %all-gather.8.cloned.1.call-start = ((), (), s32[]{:S(2)}) async-start(), calls=%async_computation.2 | async-start | bytes 7208960 | tf_op jit(solution)/shard_map/all_gather | solution.py:152
  59.3 389.0 %reduce-scatter.2.cloned.1.call-start = ((), (), s32[]{:S(2)}) async-start(), calls=%async_computation.4 | async-start | bytes 1310720 | tf_op jit(solution)/shard_map/reduce_scatter | solution.py:161
  97.1 104.0 %copy-start.8 = (f32[2048]{0:T(1024)S(1)}, f32[2048]{0:T(1024)}, u32[]{:S(2)}) copy-start(f32[2048]{0:T(1024)} %param.21) | copy-start | bytes 24580
  100.3 108.7 %copy-start.5 = (f32[3,1408]{1,0:T(4,128)S(1)}, f32[3,1408]{1,0:T(4,128)}, u32[]{:S(2)}) copy-start(f32[3,1408]{1,0:T(4,128)} %param.24) | copy-start | bytes 50692
  206.3 2.8 collective-permute-start
  207.6 5.5 %collective-permute-start.1 = (bf16[1,1408]{1,0:T(2,128)(2,1)S(1)}, bf16[1,1408]{1,0:T(2,128)(2,1)S(1)}, u32[]{:S(2)}, u32[]{:S(2)}) collective-permute-start(bf16[1,1408]{1,0:T(2,128)(2,1)S(1)} %get-tuple-element.117), channel_id=1, source_target_pairs={{4,0},{8,4},{12,8},{5,1},{9,5},{13,9},{6,2},{10,6},{14,10},{7,3},{... | collective-permute-start | bytes 8456 | tf_op jit(solution)/shard_map/ppermute | solution.py:26
Sparse Core Ops, SparseCore 0:
  57.4 35.3 all-gather.11
  94.4 106.6 all-gather.5
  202.7 104.9 all-gather.9
  309.1 104.8 all-gather.7
  425.2 23.0 reduce-scatter.1
